TPU v7x, 128 devices: a whole 4x4x4 slice. The times are simulated.
128 devices in a mesh: sp: 32 (over z, y, core), tp: 4 (over x).
Axes of the slice: x: 4, y: 4, z: 4, core: 2. Of those that a mesh axis runs over, the one named last changes fastest.
Arguments:
- query_nope: bfloat16 [6144, 4096], P('sp', 'tp'), may hold values from -6 to 6
- query_rope: bfloat16 [6144, 2048], P('sp', 'tp'), may hold values from -24 to 24
- latent: bfloat16 [6144, 512], P('sp'), may hold values from -6 to 6
- key_rope: bfloat16 [6144, 32], P('sp'), may hold values from -24 to 24
- latent_gain: float32 [512], replicated, may hold values from 0.1 to 1.9
- key_up: bfloat16 [512, 4096], P(None, 'tp'), may hold values from -0.25 to 0.25
- value_up: bfloat16 [512, 4096], P(None, 'tp'), may hold values from -0.25 to 0.25
- out_proj: bfloat16 [4096, 4096], P('tp'), may hold values from -0.09375 to 0.09375
- resid: bfloat16 [6144, 4096], P(('sp', 'tp')), may hold values from -6 to 6
- attn_gain: float32 [4096], replicated, may hold values from 0.1 to 1.9
- pre_gain: float32 [4096], replicated, may hold values from 0.1 to 1.9
- routes: int32 [6144, 2], P(('sp', 'tp')), may hold values from 0 to 31, all different within a row; in each aligned block of 48 rows (0 to 47, 48 to 95, ...) at most 6 rows name the same one
- route_weights: float32 [6144, 2], P(('sp', 'tp')), may hold values from 0.2 to 2
- expert_gate: bfloat16 [32, 4096, 1024], P('sp', None, 'tp'), may hold values from -0.09375 to 0.09375
- expert_up: bfloat16 [32, 4096, 1024], P('sp', None, 'tp'), may hold values from -0.09375 to 0.09375
- expert_down: bfloat16 [32, 1024, 4096], P('sp', 'tp'), may hold values from -0.1875 to 0.1875
- shared_gate: bfloat16 [4096, 1024], P(None, 'tp'), may hold values from -0.09375 to 0.09375
- shared_up: bfloat16 [4096, 1024], P(None, 'tp'), may hold values from -0.09375 to 0.09375
- shared_down: bfloat16 [1024, 4096], P('tp'), may hold values from -0.1875 to 0.1875
- moe_gain: float32 [4096], replicated, may hold values from 0.1 to 1.9
Outputs:
- output: bfloat16 [6144, 4096], P(('sp', 'tp'))
Inputs may be any that keep to these rules, and one draw needn't show every extreme that they name: `routes`: A row names 2 different experts. In each aligned block of 48 rows no expert is named by more than 6 rows, and in some block an expert is named by exactly 6 rows.
All inputs are finite; a program needn't handle non-finite values.
Results may differ from a plain program's by a relative error of at most 0.018.
Values may be sent and summed in bfloat16 or wider, within the bound.
No kernel may reach another device: no remote copies, remote signals or barrier semaphores. Data moves between devices by JAX's collectives and lax.ppermute only.
A program may use at most 128 MiB of HBM per device.

v0:
```python
import math
import jax
import jax.numpy as jnp
from jax import lax
from jax.sharding import PartitionSpec as P

MODEL_DIM = 4096
NOPE_DIM = 64
ROPE_DIM = 32
VALUE_DIM = 64
TOP_K = 2
epsilon = 1e-06
theta_base = 10000.0


def cut_along(array, dim, count):
    before, after = (array.shape[:dim], array.shape[dim + 1 :])
    return jnp.moveaxis(array.reshape(*before, count, -1, *after), dim, 0)


def sum_at_owner(array, axis, dim):
    count = lax.axis_size(axis)
    blocks = lax.all_to_all(cut_along(array, dim, count), axis, 0, 0, tiled=True)
    return jnp.sum(blocks.astype(jnp.float32), axis=0)


def rms_scale(values, gain_vector):
    return (
        values
        * lax.rsqrt(jnp.mean(values * values, axis=-1, keepdims=True) + epsilon)
        * gain_vector
    )


def rotate(values, positions):
    half_dim = values.shape[-1] // 2
    inverse = theta_base ** (-jnp.arange(half_dim, dtype=jnp.float32) / half_dim)
    angles = positions.astype(jnp.float32)[..., None] * inverse
    cosine = jnp.cos(angles)
    sine_part = jnp.sin(angles)
    first_half = values[..., :half_dim]
    second_half = values[..., half_dim:]
    return jnp.concatenate(
        [
            first_half * cosine - second_half * sine_part,
            second_half * cosine + first_half * sine_part,
        ],
        axis=-1,
    )


def expert_block(expert_in, gate_part, up_part, down_part):
    hidden = (
        jax.nn.silu(jnp.dot(expert_in, gate_part, preferred_element_type=jnp.float32))
        * jnp.dot(expert_in, up_part, preferred_element_type=jnp.float32)
    ).astype(jnp.bfloat16)
    return jnp.dot(hidden, down_part, preferred_element_type=jnp.float32).astype(jnp.bfloat16)


def dispatch_table(normed_rows, route_rows, experts, capacity):
    row_count = normed_rows.shape[0]
    flat_routes = route_rows.reshape(-1)
    onehot = (flat_routes[:, None] == jnp.arange(experts, dtype=jnp.int32)[None, :]).astype(
        jnp.int32
    )
    earlier = jnp.cumsum(onehot, axis=0) - onehot
    target = flat_routes * capacity + jnp.sum(earlier * onehot, axis=1)
    matches = (
        target.reshape(row_count, -1)[None, :, :]
        == jnp.arange(experts * capacity, dtype=jnp.int32)[:, None, None]
    )
    spread = jnp.any(matches, axis=2).astype(jnp.bfloat16)
    slot_table = jnp.dot(spread, normed_rows, preferred_element_type=jnp.float32).astype(
        jnp.bfloat16
    )
    return (slot_table.reshape(experts, capacity, normed_rows.shape[1]), target)


def on_device(
    query_nope,
    query_rope,
    latent,
    key_rope,
    latent_gain,
    key_up,
    value_up,
    out_proj,
    resid,
    attn_gain,
    pre_gain,
    routes,
    route_weights,
    expert_gate,
    expert_up,
    expert_down,
    shared_gate,
    shared_up,
    shared_down,
    moe_gain,
):
    local_rows = query_nope.shape[0]
    heads_here = query_nope.shape[1] // NOPE_DIM
    query_pos = lax.axis_index("sp") * local_rows + jnp.arange(local_rows, dtype=jnp.int32)
    last_query = lax.axis_index("sp") * local_rows + local_rows - 1
    query_rot = rotate(
        query_rope.astype(jnp.float32).reshape(local_rows, heads_here, ROPE_DIM), query_pos[:, None]
    ).astype(jnp.bfloat16)
    key_rot = rotate(key_rope.astype(jnp.float32), query_pos).astype(jnp.bfloat16)
    latent_normed = rms_scale(latent.astype(jnp.float32), latent_gain).astype(jnp.bfloat16)
    query_heads = query_nope.reshape(local_rows, heads_here, NOPE_DIM)
    score_scale = (NOPE_DIM + ROPE_DIM) ** (-0.5)

    def attend(state_now, latent_rows, rotary_rows, key_start):
        piece_rows = latent_rows.shape[0]
        keys_here = jnp.dot(latent_rows, key_up, preferred_element_type=jnp.float32).astype(
            jnp.bfloat16
        )
        keys_here = keys_here.reshape(piece_rows, heads_here, NOPE_DIM)
        values_here = jnp.dot(latent_rows, value_up, preferred_element_type=jnp.float32).astype(
            jnp.bfloat16
        )
        values_here = values_here.reshape(piece_rows, heads_here, VALUE_DIM)
        scores = (
            jnp.einsum("qhd,khd->hqk", query_heads, keys_here, preferred_element_type=jnp.float32)
            + jnp.einsum("qhr,kr->hqk", query_rot, rotary_rows, preferred_element_type=jnp.float32)
        ) * score_scale
        allowed = (key_start + jnp.arange(piece_rows, dtype=jnp.int32))[None, :] <= query_pos[
            :, None
        ]
        scores = jnp.where(allowed[None], scores, -1e30)
        running, total_sum, summed = state_now
        newest = jnp.maximum(running, jnp.max(scores, axis=-1))
        factor = jnp.exp(running - newest)
        exponent = jnp.exp(scores - newest[..., None])
        total_sum = total_sum * factor + jnp.sum(exponent, axis=-1)
        summed = summed * factor[..., None] + jnp.einsum(
            "hqk,khd->hqd",
            exponent.astype(jnp.bfloat16),
            values_here,
            preferred_element_type=jnp.float32,
        )
        return (newest, total_sum, summed)

    initial = (
        jnp.full((heads_here, local_rows), -1e30, jnp.float32),
        jnp.zeros((heads_here, local_rows), jnp.float32),
        jnp.zeros((heads_here, local_rows, VALUE_DIM), jnp.float32),
    )
    latent_piece = lax.all_gather(latent_normed, "sp", axis=0, tiled=True)
    rotary_piece = lax.all_gather(key_rot, "sp", axis=0, tiled=True)
    piece_rows = latent_piece.shape[0]
    step_rows = math.gcd(piece_rows, 512)

    def one_step(step_index, inner_state):
        offset = step_index * step_rows
        latent_rows = lax.dynamic_slice_in_dim(latent_piece, offset, step_rows, 0)
        rotary_rows = lax.dynamic_slice_in_dim(rotary_piece, offset, step_rows, 0)
        return lax.cond(
            offset <= last_query,
            lambda carried: attend(carried, latent_rows, rotary_rows, offset),
            lambda carried: carried,
            inner_state,
        )

    running, total_sum, summed = lax.fori_loop(0, piece_rows // step_rows, one_step, initial)
    attention = (
        (summed / total_sum[..., None])
        .transpose(1, 0, 2)
        .reshape(local_rows, heads_here * VALUE_DIM)
    )
    attention = attention.astype(jnp.bfloat16)
    projected = sum_at_owner(
        jnp.dot(attention, out_proj, preferred_element_type=jnp.float32).astype(jnp.bfloat16),
        "tp",
        0,
    )
    mixed = (resid.astype(jnp.float32) + rms_scale(projected, attn_gain)).astype(jnp.bfloat16)
    normed = rms_scale(mixed.astype(jnp.float32), pre_gain).astype(jnp.bfloat16)
    rows_here = resid.shape[0]
    tp_count = lax.axis_size("tp")
    experts = lax.axis_size("sp")
    capacity = max(2, 2 * rows_here * TOP_K // experts)
    own_table, target = dispatch_table(normed, routes, experts, capacity)
    arrived = lax.all_to_all(own_table, "sp", split_axis=0, concat_axis=0, tiled=True)
    column = lax.all_gather(arrived[None], "tp", axis=0, tiled=True)
    group_normed = lax.all_gather(normed, "tp", axis=0, tiled=True)
    expert_out = expert_block(
        column.reshape(-1, MODEL_DIM), expert_gate[0], expert_up[0], expert_down[0]
    )
    shared_part = expert_block(group_normed, shared_gate, shared_up, shared_down)
    routed_sum, shared_sum = (
        lax.psum_scatter(
            expert_out.reshape(column.shape).astype(jnp.float32).astype(jnp.bfloat16),
            "tp",
            scatter_dimension=0,
            tiled=True,
        ).astype(jnp.float32),
        lax.psum_scatter(
            shared_part.reshape(tp_count, rows_here, MODEL_DIM)
            .astype(jnp.float32)
            .astype(jnp.bfloat16),
            "tp",
            scatter_dimension=0,
            tiled=True,
        ).astype(jnp.float32),
    )
    expert_rows = lax.all_to_all(
        routed_sum.astype(jnp.bfloat16), "sp", split_axis=1, concat_axis=1, tiled=True
    ).reshape(-1, MODEL_DIM)
    shared_out = shared_sum.reshape(rows_here, MODEL_DIM)
    picked = expert_rows[target].astype(jnp.float32).reshape(rows_here, TOP_K, MODEL_DIM)
    routed = jnp.sum(picked * route_weights[..., None], axis=1)
    moe = shared_out + routed
    return (mixed.astype(jnp.float32) + rms_scale(moe, moe_gain)).astype(jnp.bfloat16)


def solution(mesh):
    in_specs = (
        P("sp", "tp"),
        P("sp", "tp"),
        P("sp", None),
        P("sp", None),
        P(),
        P(None, "tp"),
        P(None, "tp"),
        P("tp", None),
        P(("sp", "tp"), None),
        P(),
        P(),
        P(("sp", "tp"), None),
        P(("sp", "tp"), None),
        P("sp", None, "tp"),
        P("sp", None, "tp"),
        P("sp", "tp", None),
        P(None, "tp"),
        P(None, "tp"),
        P("tp", None),
        P(),
    )
    out_specs = P(("sp", "tp"), None)
    return jax.shard_map(
        on_device, mesh=mesh, in_specs=in_specs, out_specs=out_specs, check_vma=False
    )
```

profile of v0, /device:TPU:0, one launch (start us, length us, event | category | flops | bytes accessed | tf_op | source)
XLA Modules:
  0.0 656.6 jit_solution(17741494576442215457)
XLA Ops:
  6.5 1.2 fusion.42
  7.8 1.7 fusion.44
  9.5 0.7 convert_element_type.118
  10.2 1.1 copy.62
  11.3 0.7 multiply_cosine_fusion
  12.1 26.5 %all-gather.1 = bf16[32,192,32]{1,2,0:T(8,128)(2,1)S(1)} all-gather(bf16[1,192,32]{1,2,0:T(8,128)(2,1)S(1)} %maximum_bitcast_fusion), channel_id=1, replica_groups=mesh['sp'=32,'tp'=4] {'sp'}, dimensions={0}, use_global_device_ids=true | all-gather | bytes 405504 | tf_op jit(solution)/shard_map/all_gather | solution.py:150
  38.9 1.3 reshape.267
  40.2 1.0 copy.60
  41.2 0.8 subtract_convert_fusion
  42.0 19.7 %all-gather.6.cloned.1.call-done = bf16[6144,512]{1,0:T(8,128)(2,1)} async-done(((bf16[192,512]{1,0:T(8,128)(2,1)}), bf16[6144,512]{1,0:T(8,128)(2,1)}) %all-gather.6.cloned.1.call-update) | async-done | bytes 6291472 | tf_op jit(solution)/shard_map/all_gather | solution.py:149
  61.7 1.1 broadcast_in_dim.34
  62.9 22.6 %while.18 = (s32[]{:T(128)}, f32[16,192]{1,0:T(8,128)S(1)}, f32[16,192]{1,0:T(8,128)S(1)}, f32[16,192,64]{1,2,0:T(8,128)}, s32[]{:T(128)}, /*index=5*/bf16[6144,...) while((s32[]{:T(128)}, f32[16,192]{1,0:T(8,128)S(1)}, ...), condition=%wide.region_6.7_spmd.clone, body=%wide.region_1.6_spmd.clone.sunk | while | flops 1591188224 | bytes 74948008 | solution.py:165
  62.9 22.1 %conditional.3 = ((f32[16,192]{1,0:T(8,128)S(1)}, f32[16,192]{1,0:T(8,128)S(1)}, f32[16,192,64]{1,2,0:T(8,128)})) conditional(s32[]{:T(128)} %convert_element_type.188, (f32[16,192]{1,0:T(8,128)S(1)}, f32[16,192]{1,0:T(8,128)S(1)}, f32[16,192,64]{1,2,0:T(8,128)}) %tuple.60, (s32[]{:T(128)}, s32[]{:T(128)}, bf16[6144,512]{1,0:T(8,128)(2,1)}, ...), branch_computations={%region_2.0_spmd, %region_3.5_spmd} | conditional | flops 1591188224 | bytes 74946960 | solution.py:158
  62.9 3.2 convolution_convert_fusion.1
  66.1 1.5 copy.58
  67.6 2.1 fusion.59
  69.8 2.9 fusion.58
  72.7 1.6 fusion.5
  74.3 1.0 copy-done.1
  75.4 2.8 convolution_convert_fusion
  78.1 1.5 copy.59
  79.6 5.4 fusion.9
  85.5 1.3 divide_convert_fusion
  86.8 6.4 convolution_convert_fusion.5
  93.2 4.5 all-to-all-start
  98.9 20.2 %all-to-all-done = bf16[4,48,4096]{2,1,0:T(8,128)(2,1)} async-done(((bf16[4,48,4096]{2,1,0:T(8,128)(2,1)}), bf16[4,48,4096]{2,1,0:T(8,128)(2,1)}, u32[]{:S(2)}, u32[]{:S(2)}) %all-to-all-start) | async-done | bytes 1572896 | tf_op jit(solution)/shard_map/all_to_all | solution.py:23
  119.1 1.7 convert_reduce_fusion
  121.6 1.8 convolution_convert_fusion.3
  123.4 3.5 reshape.247
  126.9 275.5 %all_to_all.15 = bf16[32,6,4096]{2,1,0:T(8,128)(2,1)S(1)} all-to-all(bf16[32,6,4096]{2,1,0:T(8,128)(2,1)} %reshape.247), channel_id=1, replica_groups=mesh['sp'=32,'tp'=4] {'sp'}, dimensions={0} | all-to-all | bytes 3145728 | tf_op jit(solution)/shard_map/all_to_all | solution.py:184
  402.3 2.1 copy.66
  405.2 60.8 %all-gather.10.cloned.1.call-done = bf16[128,6,4096]{2,0,1:T(8,128)(2,1)} async-done(((bf16[32,6,4096]{2,0,1:T(8,128)(2,1)}), bf16[128,6,4096]{2,0,1:T(8,128)(2,1)}) %all-gather.10.cloned.1.call-update) | async-done | bytes 6291472 | tf_op jit(solution)/shard_map/all_gather | solution.py:185
  466.1 9.6 %copy.67 = bf16[128,6,4096]{2,1,0:T(8,128)(2,1)} copy(bf16[128,6,4096]{2,0,1:T(8,128)(2,1)} %all-gather.10.cloned.1.call-done) | data formatting | bytes 12582912 | tf_op jit(solution)/shard_map/all_gather | solution.py:185
  475.6 10.3 %reshape.248 = bf16[768,4096]{1,0:T(8,128)(2,1)} reshape(bf16[128,6,4096]{2,1,0:T(8,128)(2,1)} %copy.67) | data formatting | bytes 12582912 | tf_op jit(solution)/shard_map/reshape | solution.py:188
  486.0 6.2 fusion.22
  492.2 12.8 %convolution_convert_fusion.2 = bf16[768,4096]{1,0:T(8,128)(2,1)} fusion(bf16[1,256,4096]{2,1,0:T(8,128)(2,1)S(1)} %copy-done, bf16[768,4096]{1,0:T(8,128)(2,1)} %reshape.248, bf16[1,4096,256]{2,1,0:T(8,128)(2,1)} %param.38, f32[768,256]{1,0:T(8,128)} %fusion.22), kind=kOutput, calls=%fused_computation.25 | convolution fusion | flops 3225550848 | bytes 17563648 | tf_op jit(solution)/shard_map/dot_general | solution.py:57
  505.0 10.1 %reshape.249 = bf16[4,32,6,4096]{3,2,1,0:T(8,128)(2,1)} reshape(bf16[768,4096]{1,0:T(8,128)(2,1)} %convolution_convert_fusion.2) | data formatting | bytes 12582912 | tf_op jit(solution)/shard_map/reshape | solution.py:193
  515.4 2.6 fusion.60
  518.1 5.7 convolution_convert_fusion.4
  523.8 72.6 %reduce-scatter.5.cloned.1.call-done = bf16[1,32,6,4096]{3,2,1,0:T(8,128)(2,1)} async-done(((bf16[4,32,6,4096]{3,2,1,0:T(8,128)(2,1)}), bf16[1,32,6,4096]{3,2,1,0:T(8,128)(2,1)}) %reduce-scatter.5.cloned.1.call-update) | async-done | bytes 1572880 | tf_op jit(solution)/shard_map/reduce_scatter | solution.py:192
  596.5 7.5 %all-to-all-start.2 = ((bf16[1,32,6,4096]{3,2,0,1:T(8,128)(2,1)}), bf16[1,32,6,4096]{3,2,0,1:T(8,128)(2,1)}, u32[]{:S(2)}, u32[]{:S(2)}) async-start(bf16[1,32,6,4096]{3,2,0,1:T(8,128)(2,1)} %bitcast.77), calls=%async_computation.4 | async-start | bytes 4194304 | tf_op jit(solution)/shard_map/all_to_all | solution.py:207
  604.2 29.8 %all-to-all-done.2 = bf16[1,32,6,4096]{3,2,0,1:T(8,128)(2,1)} async-done(((bf16[1,32,6,4096]{3,2,0,1:T(8,128)(2,1)}), bf16[1,32,6,4096]{3,2,0,1:T(8,128)(2,1)}, u32[]{:S(2)}, u32[]{:S(2)}) %all-to-all-start.2) | async-done | bytes 1572896 | tf_op jit(solution)/shard_map/all_to_all | solution.py:207
  634.0 3.7 reshape.250
  637.7 3.4 gather_fusion
  641.1 2.1 reshape.255
  643.2 3.6 multiply_reduce_fusion
  646.9 1.2 multiply_reduce_fusion.1
  648.1 1.9 fusion.36
  (89 shorter events, 3.9 us)
Async XLA Ops:
  6.5 485.7 %copy-start = (bf16[1,256,4096]{2,1,0:T(8,128)(2,1)S(1)}, bf16[1,256,4096]{2,1,0:T(8,128)(2,1)}, u32[]{:S(2)}) copy-start(bf16[1,256,4096]{2,1,0:T(8,128)(2,1)} %param.39) | copy-start | bytes 6291460
  6.5 33.6 %copy-start.3 = (bf16[192,1024]{1,0:T(8,128)(2,1)S(1)}, bf16[192,1024]{1,0:T(8,128)(2,1)}, u32[]{:S(2)}) copy-start(bf16[192,1024]{1,0:T(8,128)(2,1)} %param.24) | copy-start | bytes 1179652
  6.5 55.2 %all-gather.6.cloned.1.call-start = ((), (), s32[]{:S(2)}) async-start(), calls=%async_computation.5 | async-start | bytes 6488064 | tf_op jit(solution)/shard_map/all_gather | solution.py:149
  72.6 2.7 copy-start.1
  72.7 2.7 copy-start.10
  93.2 4.7 copy-start.8
  93.2 25.9 %all-to-all-start = ((bf16[4,48,4096]{2,1,0:T(8,128)(2,1)}), bf16[4,48,4096]{2,1,0:T(8,128)(2,1)}, u32[]{:S(2)}, u32[]{:S(2)}) async-start(bf16[4,48,4096]{2,1,0:T(8,128)(2,1)} %bitcast.75), calls=%async_computation | async-start | bytes 3145728 | tf_op jit(solution)/shard_map/all_to_all | solution.py:23
  97.7 23.4 %copy-start.4 = (bf16[48,4096]{1,0:T(8,128)(2,1)S(1)}, bf16[48,4096]{1,0:T(8,128)(2,1)}, u32[]{:S(2)}) copy-start(bf16[48,4096]{1,0:T(8,128)(2,1)} %param.32) | copy-start | bytes 1179652
  97.7 23.4 %copy-start.5 = (f32[4096]{0:T(1024)S(1)}, f32[4096]{0:T(1024)}, u32[]{:S(2)}) copy-start(f32[4096]{0:T(1024)} %param.33) | copy-start | bytes 49156
  97.7 368.4 %all-gather.10.cloned.1.call-start = ((), (), s32[]{:S(2)}) async-start(), calls=%async_computation.9 | async-start | bytes 7864320 | tf_op jit(solution)/shard_map/all_gather | solution.py:185
  98.9 22.5 %copy-start.7 = (f32[4096]{0:T(1024)S(1)}, f32[4096]{0:T(1024)}, u32[]{:S(2)}) copy-start(f32[4096]{0:T(1024)} %param.34) | copy-start | bytes 49156
  121.6 5.3 copy-start.2
  404.5 111.0 %all-gather.8.cloned.1.call-start = ((), (), s32[]{:S(2)}) async-start(), calls=%async_computation.6 | async-start | bytes 1966080 | tf_op jit(solution)/shard_map/all_gather | solution.py:186
  405.2 191.3 %reduce-scatter.5.cloned.1.call-start = ((), (), s32[]{:S(2)}) async-start(), calls=%async_computation.8 | async-start | bytes 10485760 | tf_op jit(solution)/shard_map/reduce_scatter | solution.py:192
  515.1 131.7 %reduce-scatter.3.cloned.1.call-start = ((), (), s32[]{:S(2)}) async-start(), calls=%async_computation.7 | async-start | bytes 1966080 | tf_op jit(solution)/shard_map/reduce_scatter | solution.py:198
  596.5 7.6 %copy-start.9 = (f32[48,2]{0,1:T(2,128)S(1)}, f32[48,2]{0,1:T(2,128)}, u32[]{:S(2)}) copy-start(f32[48,2]{0,1:T(2,128)} %param.36) | copy-start | bytes 1156
  596.5 37.6 %all-to-all-start.2 = ((bf16[1,32,6,4096]{3,2,0,1:T(8,128)(2,1)}), bf16[1,32,6,4096]{3,2,0,1:T(8,128)(2,1)}, u32[]{:S(2)}, u32[]{:S(2)}) async-start(bf16[1,32,6,4096]{3,2,0,1:T(8,128)(2,1)} %bitcast.77), calls=%async_computation.4 | async-start | bytes 4194304 | tf_op jit(solution)/shard_map/all_to_all | solution.py:207
  643.2 4.9 copy-start.6
Sparse Core Ops, SparseCore 0:
  9.6 52.0 all-gather.5
  404.6 61.4 all-gather.9
  467.8 27.0 all-gather.7
  515.3 81.1 reduce-scatter.4
  598.7 25.3 reduce-scatter.2
where the time goes:
time: 661 us; the launch traced here: 657 us
  blocking collectives  302 us (46%)
  waiting for transfers between devices  204 us (31%)
  local copies, waits for them, and re-layouts  54.2 us (8%)
  matrix products  51.7 us (8%)
  other arithmetic  18.1 us (3%)
  between operations  13.4 us (2%)
  starting transfers between devices  12.5 us (2%)
    all_to_all x1, blocking collectives, on_device(): lax.all_to_all(own_table, 'sp', split_axis=0, concat_axis=0, tiled=True)  275 us
    reduce_scatter x1, waiting for transfers between devices, on_device(): lax.psum_scatter(expert_out.reshape(column.shape).astype(jnp.float32).ast...  72.6 us
    all_gather x1, waiting for transfers between devices, on_device(): column = lax.all_gather(arrived[None], 'tp', axis=0, tiled=True)  60.8 us
    all_to_all x1, waiting for transfers between devices, on_device(): lax.all_to_all(routed_sum.astype(jnp.bfloat16), 'sp', split_axis=1, conca...  29.8 us
    all_gather x1, blocking collectives, on_device(): rotary_piece = lax.all_gather(key_rot, 'sp', axis=0, tiled=True)  26.5 us
    all_to_all x1, waiting for transfers between devices, sum_at_owner(): lax.all_to_all(cut_along(array, dim, count), axis, 0, 0, tiled=True)  20.2 us
    all_gather x1, waiting for transfers between devices, on_device(): latent_piece = lax.all_gather(latent_normed, 'sp', axis=0, tiled=True)  19.7 us
    dot_general x2, matrix products, expert_block(): jnp.dot(hidden, down_part, preferred_element_type=jnp.float32)  18.5 us
  transfers between devices with their start and end apart: 7, of which 5 were waited for; matrix products, arithmetic and copies ran while one was open for 12% of the time, Pallas kernels for 0%

commit v1 on v0

--- a/solution.py
+++ b/solution.py
@@ -182,7 +182,9 @@
     capacity = max(2, 2 * rows_here * TOP_K // experts)
     own_table, target = dispatch_table(normed, routes, experts, capacity)
     arrived = lax.all_to_all(own_table, "sp", split_axis=0, concat_axis=0, tiled=True)
-    column = lax.all_gather(arrived[None], "tp", axis=0, tiled=True)
+    column = jnp.concatenate(
+        lax.all_to_all(jnp.stack([arrived[None]] * lax.axis_size("tp")), "tp", 0, 0), axis=0
+    )
     group_normed = lax.all_gather(normed, "tp", axis=0, tiled=True)
     expert_out = expert_block(
         column.reshape(-1, MODEL_DIM), expert_gate[0], expert_up[0], expert_down[0]

time: 661 us -> 687 us (1.039)
  waiting for transfers between devices: 204 us -> 222 us
    all_to_all x0 -> x1, waiting for transfers between devices: none -> 83.7 us  [on_device(): lax.all_to_all(jnp.stack([arrived[None]] * lax.axis_size('tp')), 'tp', 0, 0)]
    all_gather x1 -> x0, waiting for transfers between devices: 60.8 us -> none  [on_device(): column = lax.all_gather(arrived[None], 'tp', axis=0, tiled=True)]
    another operation x0 -> x2, local copies, waits for them, and re-layouts: none -> 13.7 us  [the longest x1 10.2 us: on_device(): column.reshape(-1, MODEL_DIM)]
    reshape x1 -> x0, local copies, waits for them, and re-layouts: 10.3 us -> none  [on_device(): column.reshape(-1, MODEL_DIM)]
    all_to_all x0 -> x1, local copies, waits for them, and re-layouts: none -> 9.8 us  [on_device(): lax.all_to_all(jnp.stack([arrived[None]] * lax.axis_size('tp')), 'tp', 0, 0)]
    all_gather x1 -> x0, local copies, waits for them, and re-layouts: 9.55 us -> none  [on_device(): column = lax.all_gather(arrived[None], 'tp', axis=0, tiled=True)]
  transfers between devices with their start and end apart: 7 -> 7, of which waited for: 5 -> 5; matrix products, arithmetic and copies ran while one was open for 12% -> 11% of each run, Pallas kernels for 0% -> 0%
where the time goes in v1:
time: 687 us; the launch traced here: 683 us
  blocking collectives  302 us (44%)
  waiting for transfers between devices  222 us (32%)
  local copies, waits for them, and re-layouts  56.7 us (8%)
  matrix products  52.3 us (8%)
  other arithmetic  18.1 us (3%)
  starting transfers between devices  17.8 us (3%)
  between operations  13.4 us (2%)
    all_to_all x1, blocking collectives, on_device(): lax.all_to_all(own_table, 'sp', split_axis=0, concat_axis=0, tiled=True)  276 us
    all_to_all x1, waiting for transfers between devices, on_device(): lax.all_to_all(jnp.stack([arrived[None]] * lax.axis_size('tp')), 'tp', 0, 0)  83.7 us
    reduce_scatter x1, waiting for transfers between devices, on_device(): lax.psum_scatter(expert_out.reshape(column.shape).astype(jnp.float32).ast...  67.3 us
    all_to_all x1, waiting for transfers between devices, on_device(): lax.all_to_all(routed_sum.astype(jnp.bfloat16), 'sp', split_axis=1, conca...  29.8 us
    all_gather x1, blocking collectives, on_device(): rotary_piece = lax.all_gather(key_rot, 'sp', axis=0, tiled=True)  26.5 us
    all_to_all x1, waiting for transfers between devices, sum_at_owner(): lax.all_to_all(cut_along(array, dim, count), axis, 0, 0, tiled=True)  20.3 us
    all_gather x1, waiting for transfers between devices, on_device(): latent_piece = lax.all_gather(latent_normed, 'sp', axis=0, tiled=True)  19.7 us
    dot_general x2, matrix products, expert_block(): jnp.dot(hidden, down_part, preferred_element_type=jnp.float32)  19.2 us
  transfers between devices with their start and end apart: 7, of which 5 were waited for; matrix products, arithmetic and copies ran while one was open for 11% of the time, Pallas kernels for 0%

profile of v1, /device:TPU:0, one launch (start us, length us, event | category | flops | bytes accessed | tf_op | source)
XLA Modules:
  0.0 682.7 jit_solution(4934235441943498194)
XLA Ops:
  6.5 1.2 fusion.42
  7.8 1.7 fusion.44
  10.2 1.1 copy.62
  12.1 26.5 %all-gather = bf16[32,192,32]{1,2,0:T(8,128)(2,1)S(1)} all-gather(bf16[1,192,32]{1,2,0:T(8,128)(2,1)S(1)} %maximum_bitcast_fusion), channel_id=1, replica_groups=mesh['sp'=32,'tp'=4] {'sp'}, dimensions={0}, use_global_device_ids=true | all-gather | bytes 405504 | tf_op jit(solution)/shard_map/all_gather | solution.py:150
  38.9 1.3 reshape.263
  40.2 1.0 copy.60
  41.2 0.8 subtract_convert_fusion
  42.0 19.7 %all-gather.4.cloned.1.call-done = bf16[6144,512]{1,0:T(8,128)(2,1)} async-done(((bf16[192,512]{1,0:T(8,128)(2,1)}), bf16[6144,512]{1,0:T(8,128)(2,1)}) %all-gather.4.cloned.1.call-update) | async-done | bytes 6291472 | tf_op jit(solution)/shard_map/all_gather | solution.py:149
  61.7 1.1 broadcast_in_dim.32
  62.9 22.6 %while.18 = (s32[]{:T(128)}, f32[16,192]{1,0:T(8,128)S(1)}, f32[16,192]{1,0:T(8,128)S(1)}, f32[16,192,64]{1,2,0:T(8,128)}, s32[]{:T(128)}, /*index=5*/bf16[6144,...) while((s32[]{:T(128)}, f32[16,192]{1,0:T(8,128)S(1)}, ...), condition=%wide.region_6.7_spmd.clone, body=%wide.region_1.6_spmd.clone.sunk | while | flops 1591188224 | bytes 74948008 | solution.py:165
  62.9 22.1 %conditional.3 = ((f32[16,192]{1,0:T(8,128)S(1)}, f32[16,192]{1,0:T(8,128)S(1)}, f32[16,192,64]{1,2,0:T(8,128)})) conditional(s32[]{:T(128)} %convert_element_type.188, (f32[16,192]{1,0:T(8,128)S(1)}, f32[16,192]{1,0:T(8,128)S(1)}, f32[16,192,64]{1,2,0:T(8,128)}) %tuple.60, (s32[]{:T(128)}, s32[]{:T(128)}, bf16[6144,512]{1,0:T(8,128)(2,1)}, ...), branch_computations={%region_2.0_spmd, %region_3.5_spmd} | conditional | flops 1591188224 | bytes 74946960 | solution.py:158
  62.9 3.2 convolution_convert_fusion.1
  66.1 1.5 copy.58
  67.6 2.1 fusion.59
  69.8 2.9 fusion.58
  72.7 1.6 fusion.5
  74.3 1.0 copy-done.1
  75.4 2.7 convolution_convert_fusion
  78.1 1.5 copy.59
  79.6 5.4 fusion.9
  85.5 1.3 divide_convert_fusion
  86.8 6.4 convolution_convert_fusion.5
  93.2 4.6 all-to-all-start
  98.9 20.3 %all-to-all-done = bf16[4,48,4096]{2,1,0:T(8,128)(2,1)} async-done(((bf16[4,48,4096]{2,1,0:T(8,128)(2,1)}), bf16[4,48,4096]{2,1,0:T(8,128)(2,1)}, u32[]{:S(2)}, u32[]{:S(2)}) %all-to-all-start) | async-done | bytes 1572896 | tf_op jit(solution)/shard_map/all_to_all | solution.py:23
  119.1 1.7 convert_reduce_fusion
  121.6 1.8 convolution_convert_fusion.3
  123.4 3.5 reshape.246
  126.9 275.7 %all_to_all.20 = bf16[32,6,4096]{2,1,0:T(8,128)(2,1)S(1)} all-to-all(bf16[32,6,4096]{2,1,0:T(8,128)(2,1)} %reshape.246), channel_id=1, replica_groups=mesh['sp'=32,'tp'=4] {'sp'}, dimensions={0} | all-to-all | bytes 3145728 | tf_op jit(solution)/shard_map/all_to_all | solution.py:184
  402.6 0.9 copy.66
  403.4 3.5 stack.3
  406.9 5.2 all-to-all-start.2
  413.0 83.7 %all-to-all-done.2 = bf16[4,1,32,6,4096]{4,2,3,1,0:T(8,128)(2,1)} async-done(((bf16[4,1,32,6,4096]{4,2,3,1,0:T(8,128)(2,1)}), bf16[4,1,32,6,4096]{4,2,3,1,0:T(8,128)(2,1)}, u32[]{:S(2)}, u32[]{:S(2)}) %all-to-all-start.2) | async-done | bytes 6291488 | tf_op jit(solution)/shard_map/all_to_all | solution.py:186
  496.7 9.8 %copy.67 = bf16[4,1,32,6,4096]{4,3,2,0,1:T(8,128)(2,1)} copy(bf16[4,1,32,6,4096]{4,2,3,1,0:T(8,128)(2,1)} %all-to-all-done.2) | data formatting | bytes 12582912 | tf_op jit(solution)/shard_map/all_to_all | solution.py:186
  506.5 10.2 %reshape_reshape.3 = bf16[768,4096]{1,0:T(8,128)(2,1)} reshape(bf16[4,1,32,6,4096]{4,3,2,0,1:T(8,128)(2,1)} %copy.67) | data formatting | bytes 12582912 | tf_op jit(solution)/shard_map/reshape;reshape | solution.py:190
  516.7 6.2 fusion.22
  522.9 12.8 %convolution_convert_fusion.2 = bf16[768,4096]{1,0:T(8,128)(2,1)} fusion(bf16[1,256,4096]{2,1,0:T(8,128)(2,1)S(1)} %copy-done, bf16[768,4096]{1,0:T(8,128)(2,1)} %reshape_reshape.3, bf16[1,4096,256]{2,1,0:T(8,128)(2,1)} %param.38, f32[768,256]{1,0:T(8,128)} %fusion.22), kind=kOutput, calls=%fused_computation.25 | convolution fusion | flops 3225550848 | bytes 17563648 | tf_op jit(solution)/shard_map/dot_general | solution.py:57
  535.7 10.1 %reshape.247 = bf16[4,32,6,4096]{3,2,1,0:T(8,128)(2,1)} reshape(bf16[768,4096]{1,0:T(8,128)(2,1)} %convolution_convert_fusion.2) | data formatting | bytes 12582912 | tf_op jit(solution)/shard_map/reshape | solution.py:195
  546.1 2.6 fusion.60
  548.8 6.4 convolution_convert_fusion.4
  555.2 67.3 %reduce-scatter.5.cloned.1.call-done = bf16[1,32,6,4096]{3,2,1,0:T(8,128)(2,1)} async-done(((bf16[4,32,6,4096]{3,2,1,0:T(8,128)(2,1)}), bf16[1,32,6,4096]{3,2,1,0:T(8,128)(2,1)}) %reduce-scatter.5.cloned.1.call-update) | async-done | bytes 1572880 | tf_op jit(solution)/shard_map/reduce_scatter | solution.py:194
  622.5 7.5 %all-to-all-start.3 = ((bf16[1,32,6,4096]{3,2,0,1:T(8,128)(2,1)}), bf16[1,32,6,4096]{3,2,0,1:T(8,128)(2,1)}, u32[]{:S(2)}, u32[]{:S(2)}) async-start(bf16[1,32,6,4096]{3,2,0,1:T(8,128)(2,1)} %bitcast.79), calls=%async_computation.5 | async-start | bytes 4194304 | tf_op jit(solution)/shard_map/all_to_all | solution.py:209
  630.3 29.8 %all-to-all-done.3 = bf16[1,32,6,4096]{3,2,0,1:T(8,128)(2,1)} async-done(((bf16[1,32,6,4096]{3,2,0,1:T(8,128)(2,1)}), bf16[1,32,6,4096]{3,2,0,1:T(8,128)(2,1)}, u32[]{:S(2)}, u32[]{:S(2)}) %all-to-all-start.3) | async-done | bytes 1572896 | tf_op jit(solution)/shard_map/all_to_all | solution.py:209
  660.1 3.7 reshape.248
  663.8 3.4 gather_fusion
  667.2 2.1 reshape.253
  669.3 3.6 multiply_reduce_fusion
  673.0 1.2 multiply_reduce_fusion.1
  674.2 1.9 fusion.36
  (89 shorter events, 5.1 us)
Async XLA Ops:
  6.5 516.4 %copy-start = (bf16[1,256,4096]{2,1,0:T(8,128)(2,1)S(1)}, bf16[1,256,4096]{2,1,0:T(8,128)(2,1)}, u32[]{:S(2)}) copy-start(bf16[1,256,4096]{2,1,0:T(8,128)(2,1)} %param.39) | copy-start | bytes 6291460
  6.5 33.6 %copy-start.3 = (bf16[192,1024]{1,0:T(8,128)(2,1)S(1)}, bf16[192,1024]{1,0:T(8,128)(2,1)}, u32[]{:S(2)}) copy-start(bf16[192,1024]{1,0:T(8,128)(2,1)} %param.24) | copy-start | bytes 1179652
  6.5 55.2 %all-gather.4.cloned.1.call-start = ((), (), s32[]{:S(2)}) async-start(), calls=%async_computation.6 | async-start | bytes 6488064 | tf_op jit(solution)/shard_map/all_gather | solution.py:149
  72.7 2.7 copy-start.1
  72.7 2.7 copy-start.10
  93.2 4.7 copy-start.8
  93.2 25.9 %all-to-all-start = ((bf16[4,48,4096]{2,1,0:T(8,128)(2,1)}), bf16[4,48,4096]{2,1,0:T(8,128)(2,1)}, u32[]{:S(2)}, u32[]{:S(2)}) async-start(bf16[4,48,4096]{2,1,0:T(8,128)(2,1)} %bitcast.77), calls=%async_computation | async-start | bytes 3145728 | tf_op jit(solution)/shard_map/all_to_all | solution.py:23
  97.9 23.2 %copy-start.4 = (bf16[48,4096]{1,0:T(8,128)(2,1)S(1)}, bf16[48,4096]{1,0:T(8,128)(2,1)}, u32[]{:S(2)}) copy-start(bf16[48,4096]{1,0:T(8,128)(2,1)} %param.32) | copy-start | bytes 1179652
  97.9 23.2 %copy-start.5 = (f32[4096]{0:T(1024)S(1)}, f32[4096]{0:T(1024)}, u32[]{:S(2)}) copy-start(f32[4096]{0:T(1024)} %param.33) | copy-start | bytes 49156
  98.9 22.6 %copy-start.7 = (f32[4096]{0:T(1024)S(1)}, f32[4096]{0:T(1024)}, u32[]{:S(2)}) copy-start(f32[4096]{0:T(1024)} %param.34) | copy-start | bytes 49156
  121.6 5.3 copy-start.2
  406.9 89.8 %all-to-all-start.2 = ((bf16[4,1,32,6,4096]{4,2,3,1,0:T(8,128)(2,1)}), bf16[4,1,32,6,4096]{4,2,3,1,0:T(8,128)(2,1)}, u32[]{:S(2)}, u32[]{:S(2)}) async-start(bf16[4,1,32,6,4096]{4,2,3,1,0:T(8,128)(2,1)} %stack.3), calls=%async_computation.3 | async-start | bytes 12582912 | tf_op jit(solution)/shard_map/all_to_all | solution.py:186
  412.2 134.0 %all-gather.6.cloned.1.call-start = ((), (), s32[]{:S(2)}) async-start(), calls=%async_computation.7 | async-start | bytes 1966080 | tf_op jit(solution)/shard_map/all_gather | solution.py:188
  412.9 209.6 %reduce-scatter.5.cloned.1.call-start = ((), (), s32[]{:S(2)}) async-start(), calls=%async_computation.9 | async-start | bytes 10485760 | tf_op jit(solution)/shard_map/reduce_scatter | solution.py:194
  545.8 127.1 %reduce-scatter.3.cloned.1.call-start = ((), (), s32[]{:S(2)}) async-start(), calls=%async_computation.8 | async-start | bytes 1966080 | tf_op jit(solution)/shard_map/reduce_scatter | solution.py:200
  622.5 7.7 %copy-start.9 = (f32[48,2]{0,1:T(2,128)S(1)}, f32[48,2]{0,1:T(2,128)}, u32[]{:S(2)}) copy-start(f32[48,2]{0,1:T(2,128)} %param.36) | copy-start | bytes 1156
  622.5 37.6 %all-to-all-start.3 = ((bf16[1,32,6,4096]{3,2,0,1:T(8,128)(2,1)}), bf16[1,32,6,4096]{3,2,0,1:T(8,128)(2,1)}, u32[]{:S(2)}, u32[]{:S(2)}) async-start(bf16[1,32,6,4096]{3,2,0,1:T(8,128)(2,1)} %bitcast.79), calls=%async_computation.5 | async-start | bytes 4194304 | tf_op jit(solution)/shard_map/all_to_all | solution.py:209
  669.3 4.9 copy-start.6
Sparse Core Ops, SparseCore 0:
  9.6 52.0 all-gather.3
  414.6 37.0 all-gather.5
  546.0 76.5 reduce-scatter.4
  624.8 25.3 reduce-scatter.2
